TPU v7x, 512 devices: a whole 4x8x8 slice. The times are simulated.
512 devices in a mesh: ep: 128 (over z, y, core), tp: 4 (over x).
Axes of the slice: x: 4, y: 8, z: 8, core: 2. Of those that a mesh axis runs over, the one named last changes fastest.
Arguments:
- tokens: bfloat16 [2048, 1024], P('ep', 'tp'), may hold values from -75 to 75
- gain_mix: float32 [1024], replicated, may hold values from 0.1 to 1.9
- w_query: bfloat16 [1024, 512], P(None, 'tp'), may hold values from -0.1875 to 0.1875
- w_key: bfloat16 [1024, 512], P(None, 'tp'), may hold values from -0.1875 to 0.1875
- w_value: bfloat16 [1024, 512], P(None, 'tp'), may hold values from -0.1875 to 0.1875
- w_outgate: bfloat16 [1024, 512], P(None, 'tp'), may hold values from -0.1875 to 0.1875
- w_input_gate: bfloat16 [1024, 4], P(None, 'tp'), may hold values from -0.1875 to 0.1875
- w_forget_gate: bfloat16 [1024, 4], P(None, 'tp'), may hold values from -0.1875 to 0.1875
- w_mix_out: bfloat16 [512, 1024], P(None, 'tp'), may hold values from -0.25 to 0.25
- cell_state: float32 [2048, 4, 128, 128], P('ep', 'tp'), may hold values from -3 to 3
- norm_state: float32 [2048, 4, 128], P('ep', 'tp'), may hold values from -3 to 3
- max_state: float32 [2048, 4], P('ep', 'tp'), may hold values from -2 to 143
- gain_ffn: float32 [1024], replicated, may hold values from 0.1 to 1.9
- route_ids: int32 [2048, 2], P('ep'), may hold values from 0 to 127, all different within a row; in each aligned block of 16 rows (0 to 15, 16 to 31, ...) no two rows name the same one
- route_logits: float32 [2048, 2], P('ep'), may hold values from -5 to 5
- expert_gate: bfloat16 [128, 1024, 1408], P('ep', None, 'tp'), may hold values from -0.1875 to 0.1875
- expert_up: bfloat16 [128, 1024, 1408], P('ep', None, 'tp'), may hold values from -0.1875 to 0.1875
- expert_down: bfloat16 [128, 1408, 1024], P('ep', 'tp'), may hold values from -0.15625 to 0.15625
- dense_gate: bfloat16 [1024, 3072], P('tp', 'ep'), may hold values from -0.1875 to 0.1875
- dense_up: bfloat16 [1024, 3072], P('tp', 'ep'), may hold values from -0.1875 to 0.1875
- dense_down: bfloat16 [3072, 1024], P('ep', 'tp'), may hold values from -0.3125 to 0.3125
- dense_mix: bfloat16 [1024], P('tp'), may hold values from -0.1875 to 0.1875
Outputs:
- layer_out: bfloat16 [2048, 1024], P('ep', 'tp')
Inputs may be any that keep to these rules, and one draw needn't show every extreme that they name: `route_ids`: each row names 2 different experts. Among the 16 tokens of one index of ep no expert is named more than 1 times, and in every draw some expert is named exactly 1 times by the tokens of one index of ep.
All inputs are finite; a program needn't handle non-finite values.
Results may differ from a plain program's by a relative error of at most 0.013.
Values may be sent and summed in bfloat16 or wider, within the bound.
No kernel may reach another device: no remote copies, remote signals or barrier semaphores. Data moves between devices by JAX's collectives and lax.ppermute only.
A program may use at most 64 MiB of HBM per device.

v0:
```python
import jax
import jax.numpy as jnp
from jax import lax
from jax.sharding import PartitionSpec as P

HEAD = 128
TOP = 2
epsilon = 1e-06
highest = lax.Precision.HIGHEST


def sent_to_all(shard, axis):
    size = lax.axis_size(axis)
    return lax.all_to_all(
        jnp.broadcast_to(shard[None], (size, *shard.shape)), axis, 0, 0, tiled=True
    )


def joined_along(blocks, dim):
    dims = list(blocks.shape[1:])
    dims[dim] *= blocks.shape[0]
    return jnp.moveaxis(blocks, 0, dim).reshape(dims)


def collect(shard, axis, dim):
    blocks = sent_to_all(shard, axis)
    return joined_along(blocks, dim)


def cut_along(shard, dim, size):
    dims = shard.shape
    blocks = shard.reshape(*dims[:dim], size, dims[dim] // size, *dims[dim + 1 :])
    return jnp.moveaxis(blocks, dim, 0)


def sent_and_summed(shard, axis, dim):
    blocks = cut_along(shard, dim, lax.axis_size(axis))
    arrived = lax.all_to_all(blocks, axis, split_axis=0, concat_axis=0, tiled=True)
    return arrived.astype(jnp.float32).sum(axis=0)


def turned_gather(arrays, axis, dims):
    turned = [jnp.moveaxis(a, dim, 0) for a, dim in zip(arrays, dims)]
    widths = [t[0].size for t in turned]
    both = jnp.concatenate([t.reshape(-1, w) for t, w in zip(turned, widths)], axis=1)
    result = lax.all_gather(both, axis, axis=0, tiled=True)
    blocks = jnp.split(result, [sum(widths[:k]) for k in range(1, len(widths))], axis=1)
    return tuple(
        (
            jnp.moveaxis(b.reshape(-1, *t.shape[1:]), 0, dim)
            for b, t, dim in zip(blocks, turned, dims)
        )
    )


def of_everyone(shard, axis):
    return sent_to_all(shard, axis).astype(jnp.float32).sum(axis=0)


def rms_norm(rows, gain):
    values = rows.astype(jnp.float32)
    scale = lax.rsqrt(jnp.mean(values * values, axis=-1, keepdims=True) + epsilon)
    return (values * scale * gain).astype(jnp.bfloat16)


def local(
    tokens,
    gain_mix,
    w_query,
    w_key,
    w_value,
    w_outgate,
    w_input_gate,
    w_forget_gate,
    w_mix_out,
    cell_state,
    norm_state,
    max_state,
    gain_ffn,
    route_ids,
    route_logits,
    expert_gate,
    expert_up,
    expert_down,
    dense_gate,
    dense_up,
    dense_down,
    dense_mix,
):
    seq_count, quarter = tokens.shape
    tp_rank = lax.axis_index("tp")
    full_tokens = collect(tokens, "tp", 1)
    normed_mix = rms_norm(full_tokens, gain_mix)

    def project(weight):
        return jnp.dot(normed_mix, weight, preferred_element_type=jnp.float32)

    query_rows = project(w_query).reshape(seq_count, -1, HEAD)
    key_rows = project(w_key).reshape(seq_count, -1, HEAD) * HEAD ** (-0.5)
    value_rows = project(w_value).reshape(seq_count, -1, HEAD)
    out_gate = project(w_outgate)
    input_gate = project(w_input_gate)
    carried = jax.nn.log_sigmoid(project(w_forget_gate)) + max_state
    stabilizer = jnp.maximum(carried, input_gate)
    weight_old = jnp.exp(carried - stabilizer)
    weight_new = jnp.exp(input_gate - stabilizer) * jnp.sum(query_rows * key_rows, axis=-1)
    cell_read = jnp.einsum("bhd,bhde->bhe", query_rows, cell_state, precision=highest)
    numerator = weight_old[..., None] * cell_read + weight_new[..., None] * value_rows
    denominator = weight_old * jnp.sum(query_rows * norm_state, axis=-1) + weight_new
    cell_out = numerator / jnp.maximum(jnp.abs(denominator), 1.0)[..., None]
    mixed = (jax.nn.sigmoid(out_gate) * cell_out.reshape(seq_count, -1)).astype(jnp.bfloat16)
    all_heads = collect(mixed, "tp", 1)
    resid = (
        tokens.astype(jnp.float32)
        + jnp.dot(all_heads, w_mix_out, preferred_element_type=jnp.float32)
    ).astype(jnp.bfloat16)
    whole_resid = collect(resid, "tp", 1)
    normed_full = rms_norm(whole_resid, gain_ffn)
    normed_part = lax.dynamic_slice_in_dim(normed_full, tp_rank * quarter, quarter, 1)
    experts = lax.axis_size("ep")
    slots = (2 * seq_count * TOP + experts - 1) // experts
    flat_ids = route_ids.reshape(-1)
    onehot = (flat_ids[:, None] == jnp.arange(experts, dtype=jnp.int32)[None, :]).astype(jnp.int32)
    earlier = jnp.cumsum(onehot, axis=0) - onehot
    slot_rank = jnp.sum(earlier * onehot, axis=1)
    target = flat_ids * slots + slot_rank
    select = (jnp.arange(experts * slots, dtype=jnp.int32)[:, None] == target[None, :]).astype(
        jnp.bfloat16
    )
    repeated = jnp.repeat(normed_full, TOP, axis=0)
    outgoing = jnp.dot(select, repeated, preferred_element_type=jnp.float32).astype(jnp.bfloat16)
    outgoing = outgoing.reshape(experts, slots, -1)
    received = lax.all_to_all(outgoing, "ep", split_axis=0, concat_axis=0, tiled=True)
    sources = received.shape[0]
    item_count = received.shape[1]
    flat_rows = received.reshape(sources * item_count, -1)
    gate_rows = jnp.dot(flat_rows, expert_gate[0], preferred_element_type=jnp.float32)
    up_rows = jnp.dot(flat_rows, expert_up[0], preferred_element_type=jnp.float32)
    hidden = (jax.nn.silu(gate_rows) * up_rows).astype(jnp.bfloat16)
    partial_value = jnp.dot(hidden, expert_down[0], preferred_element_type=jnp.float32)
    summed = sent_and_summed(partial_value.astype(jnp.bfloat16), "tp", 1).astype(jnp.bfloat16)
    returned = lax.all_to_all(
        summed.reshape(sources, item_count, -1), "ep", split_axis=0, concat_axis=0, tiled=True
    )
    picked = lax.dot_general(
        select,
        returned.reshape(experts * slots, -1),
        (((0,), (0,)), ((), ())),
        preferred_element_type=jnp.float32,
    ).reshape(seq_count, TOP, -1)
    route_weight = jax.nn.sigmoid(route_logits - route_logits[:, ::-1])
    moe = jnp.sum(route_weight[..., None] * picked, axis=1)
    mix_part = jnp.dot(normed_part, dense_mix, preferred_element_type=jnp.float32)
    pieces = turned_gather((dense_gate, dense_up), "ep", (1, 1))
    gate_cols = jnp.dot(normed_part, pieces[0], preferred_element_type=jnp.float32)
    up_cols = jnp.dot(normed_part, pieces[1], preferred_element_type=jnp.float32)
    gate_sum, up_sum, mix_logit = (
        of_everyone(gate_cols.astype(jnp.bfloat16), "tp").astype(jnp.float32),
        of_everyone(up_cols.astype(jnp.bfloat16), "tp").astype(jnp.float32),
        of_everyone(mix_part.astype(jnp.bfloat16), "tp").astype(jnp.float32),
    )
    dense_hidden = (jax.nn.silu(gate_sum) * up_sum).astype(jnp.bfloat16)
    dense_out = jnp.dot(
        dense_hidden,
        lax.all_gather(dense_down, "ep", axis=0, tiled=True),
        preferred_element_type=jnp.float32,
    )
    mix_gate = jax.nn.sigmoid(mix_logit)
    total = resid.astype(jnp.float32) + moe + mix_gate[:, None] * dense_out
    return total.astype(jnp.bfloat16)


def solution(mesh):
    return jax.shard_map(
        local,
        mesh=mesh,
        in_specs=(
            P("ep", "tp"),
            P(),
            P(None, "tp"),
            P(None, "tp"),
            P(None, "tp"),
            P(None, "tp"),
            P(None, "tp"),
            P(None, "tp"),
            P(None, "tp"),
            P("ep", "tp", None, None),
            P("ep", "tp", None),
            P("ep", "tp"),
            P(),
            P("ep", None),
            P("ep", None),
            P("ep", None, "tp"),
            P("ep", None, "tp"),
            P("ep", "tp", None),
            P("tp", "ep"),
            P("tp", "ep"),
            P("ep", "tp"),
            P("tp"),
        ),
        out_specs=P("ep", "tp"),
        check_vma=False,
    )
```

profile of v0, /device:TPU:1, one launch (start us, length us, event | category | flops | bytes accessed | tf_op | source)
XLA Modules:
  0.0 192.4 jit_solution(7491865044756722748)
XLA Ops:
  6.6 1.4 pad_maximum_fusion
  8.0 1.3 broadcast_in_dim.14
  9.3 4.8 %all-to-all-start = ((bf16[4,16,256]{2,1,0:T(8,128)(2,1)}), bf16[4,16,256]{2,1,0:T(8,128)(2,1)S(1)}, u32[]{:S(2)}, u32[]{:S(2)}) async-start(bf16[4,16,256]{2,1,0:T(8,128)(2,1)} %broadcast_in_dim.14), calls=%async_computation | async-start | bytes 65536 | tf_op jit(solution)/shard_map/all_to_all | solution.py:14
  14.2 0.7 all-gather.5.cloned.1.call-update
  14.9 0.7 mul.148
  15.6 0.8 copy.72
  16.5 2.0 %all-to-all-done = bf16[4,16,256]{2,1,0:T(8,128)(2,1)S(1)} async-done(((bf16[4,16,256]{2,1,0:T(8,128)(2,1)}), bf16[4,16,256]{2,1,0:T(8,128)(2,1)S(1)}, u32[]{:S(2)}, u32[]{:S(2)}) %all-to-all-start) | async-done | bytes 32800 | tf_op jit(solution)/shard_map/all_to_all | solution.py:14
  18.6 0.8 multiply_convert_fusion.3
  19.5 1.1 fusion.14
  20.6 1.2 fusion.51
  21.8 1.2 fusion.16
  23.1 1.0 fusion.19
  24.5 0.6 broadcast_in_dim.15
  25.1 3.2 %all-to-all-start.1 = ((bf16[4,16,128]{2,1,0:T(8,128)(2,1)}), bf16[4,16,128]{2,1,0:T(8,128)(2,1)S(1)}, u32[]{:S(2)}, u32[]{:S(2)}) async-start(bf16[4,16,128]{2,1,0:T(8,128)(2,1)} %broadcast_in_dim.15), calls=%async_computation.1 | async-start | bytes 32768 | tf_op jit(solution)/shard_map/all_to_all | solution.py:14
  28.5 4.0 %all-to-all-done.1 = bf16[4,16,128]{2,1,0:T(8,128)(2,1)S(1)} async-done(((bf16[4,16,128]{2,1,0:T(8,128)(2,1)}), bf16[4,16,128]{2,1,0:T(8,128)(2,1)S(1)}, u32[]{:S(2)}, u32[]{:S(2)}) %all-to-all-start.1) | async-done | bytes 16416 | tf_op jit(solution)/shard_map/all_to_all | solution.py:14
  32.7 0.6 broadcast_in_dim.16
  33.3 3.3 %all-to-all-start.2 = ((bf16[4,16,256]{2,1,0:T(8,128)(2,1)}), bf16[4,16,256]{2,1,0:T(8,128)(2,1)S(1)}, u32[]{:S(2)}, u32[]{:S(2)}) async-start(bf16[4,16,256]{2,1,0:T(8,128)(2,1)} %broadcast_in_dim.16), calls=%async_computation.2 | async-start | bytes 65536 | tf_op jit(solution)/shard_map/all_to_all | solution.py:14
  36.6 0.2 select_reduce_fusion
  36.8 4.1 %all-to-all-done.2 = bf16[4,16,256]{2,1,0:T(8,128)(2,1)S(1)} async-done(((bf16[4,16,256]{2,1,0:T(8,128)(2,1)}), bf16[4,16,256]{2,1,0:T(8,128)(2,1)S(1)}, u32[]{:S(2)}, u32[]{:S(2)}) %all-to-all-start.2) | async-done | bytes 32800 | tf_op jit(solution)/shard_map/all_to_all | solution.py:14
  41.2 0.2 fusion.2
  41.4 0.5 broadcast.120
  41.9 0.7 reduce.9
  42.6 0.9 reshape.195
  43.5 21.3 %all-to-all-start.3 = ((bf16[128,2,512]{2,1,0:T(2,128)(2,1)}), bf16[128,2,512]{2,1,0:T(2,128)(2,1)S(1)}, u32[]{:S(2)}, u32[]{:S(2)}) async-start(bf16[128,2,512]{2,1,0:T(2,128)(2,1)} %reshape.195), calls=%async_computation.3 | async-start | bytes 524288 | tf_op jit(solution)/shard_map/all_to_all | solution.py:133
  65.0 15.1 %all-to-all-done.3 = bf16[128,2,512]{2,1,0:T(2,128)(2,1)S(1)} async-done(((bf16[128,2,512]{2,1,0:T(2,128)(2,1)}), bf16[128,2,512]{2,1,0:T(2,128)(2,1)S(1)}, u32[]{:S(2)}, u32[]{:S(2)}) %all-to-all-start.3) | async-done | bytes 262176 | tf_op jit(solution)/shard_map/all_to_all | solution.py:133
  80.0 0.2 reshape.196
  80.3 0.4 fusion.24
  80.7 2.0 %convolution_convert_fusion.3 = bf16[128,1024]{1,0:T(8,128)(2,1)S(1)} fusion(bf16[1,352,1024]{2,1,0:T(8,128)(2,1)S(1)} %copy-done.6, bf16[1,1024,352]{1,2,0:T(8,128)(2,1)} %param.38, f32[128,352]{0,1:T(8,128)S(1)} %fusion.24, bf16[128,1,1024]{2,1,0:T(2,128)(2,1)S(1)} %reshape.196), kind=kOutput, calls=%fused_computation.5 | convolution fusion | flops 184950784 | bytes 2146304 | tf_op jit(solution)/shard_map/dot_general | solution.py:140
  82.7 0.7 copy.109
  83.4 3.4 %all-to-all-start.4 = ((bf16[4,128,256]{2,1,0:T(8,128)(2,1)}), bf16[4,128,256]{2,1,0:T(8,128)(2,1)S(1)}, u32[]{:S(2)}, u32[]{:S(2)}) async-start(bf16[4,128,256]{2,1,0:T(8,128)(2,1)} %bitcast.113), calls=%async_computation.4 | async-start | bytes 524288 | tf_op jit(solution)/shard_map/all_to_all | solution.py:38
  87.0 6.0 %all-to-all-done.4 = bf16[4,128,256]{2,1,0:T(8,128)(2,1)S(1)} async-done(((bf16[4,128,256]{2,1,0:T(8,128)(2,1)}), bf16[4,128,256]{2,1,0:T(8,128)(2,1)S(1)}, u32[]{:S(2)}, u32[]{:S(2)}) %all-to-all-start.4) | async-done | bytes 262176 | tf_op jit(solution)/shard_map/all_to_all | solution.py:38
  92.9 0.6 broadcast_in_dim.18
  93.5 3.2 %all-to-all-start.6 = ((bf16[4,1,16]{2,1,0:T(2,128)(2,1)}), bf16[4,1,16]{2,1,0:T(2,128)(2,1)S(1)}, u32[]{:S(2)}, u32[]{:S(2)}) async-start(bf16[4,1,16]{2,1,0:T(2,128)(2,1)} %broadcast_in_dim.18), calls=%async_computation.6 | async-start | bytes 4096 | tf_op jit(solution)/shard_map/all_to_all | solution.py:14
  96.8 0.6 reduce.10
  97.4 0.6 reshape.197
  98.0 2.8 %all-to-all-done.6 = bf16[4,1,16]{2,1,0:T(2,128)(2,1)S(1)} async-done(((bf16[4,1,16]{2,1,0:T(2,128)(2,1)}), bf16[4,1,16]{2,1,0:T(2,128)(2,1)S(1)}, u32[]{:S(2)}, u32[]{:S(2)}) %all-to-all-start.6) | async-done | bytes 160 | tf_op jit(solution)/shard_map/all_to_all | solution.py:14
  100.7 7.7 %all-to-all-start.5 = ((bf16[128,2,128]{2,1,0:T(2,128)(2,1)}), bf16[128,2,128]{2,1,0:T(2,128)(2,1)S(1)}, u32[]{:S(2)}, u32[]{:S(2)}) async-start(bf16[128,2,128]{2,1,0:T(2,128)(2,1)} %reshape.197), calls=%async_computation.5 | async-start | bytes 131072 | tf_op jit(solution)/shard_map/all_to_all | solution.py:142
  108.5 1.9 convolution_convert_fusion.1
  110.4 9.6 %all-to-all-done.5 = bf16[128,2,128]{2,1,0:T(2,128)(2,1)S(1)} async-done(((bf16[128,2,128]{2,1,0:T(2,128)(2,1)}), bf16[128,2,128]{2,1,0:T(2,128)(2,1)S(1)}, u32[]{:S(2)}, u32[]{:S(2)}) %all-to-all-start.5) | async-done | bytes 65568 | tf_op jit(solution)/shard_map/all_to_all | solution.py:142
  120.0 0.8 broadcast_in_dim.19
  120.8 3.5 %all-to-all-start.7 = ((bf16[4,16,3072]{2,1,0:T(8,128)(2,1)}), bf16[4,16,3072]{2,1,0:T(8,128)(2,1)S(1)}, u32[]{:S(2)}, u32[]{:S(2)}) async-start(bf16[4,16,3072]{2,1,0:T(8,128)(2,1)} %broadcast_in_dim.19), calls=%async_computation.7 | async-start | bytes 786432 | tf_op jit(solution)/shard_map/all_to_all | solution.py:14
  124.3 1.9 convolution_convert_fusion
  126.2 5.6 %all-to-all-done.7 = bf16[4,16,3072]{2,1,0:T(8,128)(2,1)S(1)} async-done(((bf16[4,16,3072]{2,1,0:T(8,128)(2,1)}), bf16[4,16,3072]{2,1,0:T(8,128)(2,1)S(1)}, u32[]{:S(2)}, u32[]{:S(2)}) %all-to-all-start.7) | async-done | bytes 393248 | tf_op jit(solution)/shard_map/all_to_all | solution.py:14
  131.9 0.8 broadcast_in_dim.20
  132.6 3.5 %all-to-all-start.8 = ((bf16[4,16,3072]{2,1,0:T(8,128)(2,1)}), bf16[4,16,3072]{2,1,0:T(8,128)(2,1)S(1)}, u32[]{:S(2)}, u32[]{:S(2)}) async-start(bf16[4,16,3072]{2,1,0:T(8,128)(2,1)} %broadcast_in_dim.20), calls=%async_computation.8 | async-start | bytes 786432 | tf_op jit(solution)/shard_map/all_to_all | solution.py:14
  136.3 6.2 %all-to-all-done.8 = bf16[4,16,3072]{2,1,0:T(8,128)(2,1)S(1)} async-done(((bf16[4,16,3072]{2,1,0:T(8,128)(2,1)}), bf16[4,16,3072]{2,1,0:T(8,128)(2,1)S(1)}, u32[]{:S(2)}, u32[]{:S(2)}) %all-to-all-start.8) | async-done | bytes 393248 | tf_op jit(solution)/shard_map/all_to_all | solution.py:14
  142.6 40.6 %all-gather.5.cloned.1.call-done = bf16[3072,256]{1,0:T(8,128)(2,1)} async-done(((bf16[24,256]{1,0:T(8,128)(2,1)}), bf16[3072,256]{1,0:T(8,128)(2,1)}) %all-gather.5.cloned.1.call-update) | async-done | bytes 1572880 | tf_op jit(solution)/shard_map/all_gather | solution.py:165
  183.3 2.3 %fusion.7 = bf16[16,256]{1,0:T(8,128)(2,1)} fusion(bf16[3072,256]{1,0:T(8,128)(2,1)} %all-gather.5.cloned.1.call-done, f32[16,3072]{1,0:T(8,128)S(1)} %convert_reduce_fusion, f32[16,3072]{1,0:T(8,128)S(1)} %convert_reduce_fusion.1, f32[16,256]{1,0:T(8,128)S(1)} %fusion.4, bf16[16,256]{1,0:T(8,128)(2,1)S(1)} %fusion.6, f32[16]{0:T(128)S(1)} %add_divide_fusion.1), kind=kOutput, calls=%fused_computation.15 | convolution fusion | flops 25481216 | bytes 1998912 | tf_op jit(solution)/shard_map/dot_general | solution.py:163
  (62 shorter events, 2.0 us)
Async XLA Ops:
  6.5 16.5 %copy-start = (f32[16,1,128,128]{3,2,1,0:T(8,128)S(1)}, f32[16,1,128,128]{3,2,1,0:T(8,128)}, u32[]{:S(2)}) copy-start(f32[16,1,128,128]{3,2,1,0:T(8,128)} %param.31) | copy-start | bytes 3145732
  6.5 17.5 %copy-start.8 = (bf16[1024,1]{0,1:T(2,128)(2,1)S(1)}, bf16[1024,1]{0,1:T(2,128)(2,1)}, u32[]{:S(2)}) copy-start(bf16[1024,1]{0,1:T(2,128)(2,1)} %param.29) | copy-start | bytes 6148
  6.5 17.5 %copy-start.10 = (f32[16,1]{0,1:T(1,128)S(1)}, f32[16,1]{0,1:T(1,128)}, u32[]{:S(2)}) copy-start(f32[16,1]{0,1:T(1,128)} %param.33) | copy-start | bytes 196
  6.5 17.6 %copy-start.9 = (bf16[1024,1]{0,1:T(2,128)(2,1)S(1)}, bf16[1024,1]{0,1:T(2,128)(2,1)}, u32[]{:S(2)}) copy-start(bf16[1024,1]{0,1:T(2,128)(2,1)} %param.28) | copy-start | bytes 6148
  6.5 17.8 %copy-start.7 = (bf16[1024,128]{1,0:T(8,128)(2,1)S(1)}, bf16[1024,128]{1,0:T(8,128)(2,1)}, u32[]{:S(2)}) copy-start(bf16[1024,128]{1,0:T(8,128)(2,1)} %param.26) | copy-start | bytes 786436
  6.5 101.9 %all-gather.3.cloned.1.call-start = ((), (), s32[]{:S(2)}) async-start(), calls=%async_computation.9 | async-start | bytes 3170304 | tf_op jit(solution)/shard_map/all_gather | solution.py:46
  9.3 9.1 %all-to-all-start = ((bf16[4,16,256]{2,1,0:T(8,128)(2,1)}), bf16[4,16,256]{2,1,0:T(8,128)(2,1)S(1)}, u32[]{:S(2)}, u32[]{:S(2)}) async-start(bf16[4,16,256]{2,1,0:T(8,128)(2,1)} %broadcast_in_dim.14), calls=%async_computation | async-start | bytes 65536 | tf_op jit(solution)/shard_map/all_to_all | solution.py:14
  14.2 18.4 %copy-start.2 = (bf16[512,256]{1,0:T(8,128)(2,1)S(1)}, bf16[512,256]{1,0:T(8,128)(2,1)}, u32[]{:S(2)}) copy-start(bf16[512,256]{1,0:T(8,128)(2,1)} %param.30) | copy-start | bytes 786436
  14.2 18.4 %copy-start.3 = (bf16[16,256]{1,0:T(8,128)(2,1)S(1)}, bf16[16,256]{1,0:T(8,128)(2,1)}, u32[]{:S(2)}) copy-start(bf16[16,256]{1,0:T(8,128)(2,1)} %param.22) | copy-start | bytes 24580
  14.2 169.1 %all-gather.5.cloned.1.call-start = ((), (), s32[]{:S(2)}) async-start(), calls=%async_computation.10 | async-start | bytes 1585152 | tf_op jit(solution)/shard_map/all_gather | solution.py:165
  19.5 21.5 %copy-start.4 = (f32[1024]{0:T(1024)S(1)}, f32[1024]{0:T(1024)}, u32[]{:S(2)}) copy-start(f32[1024]{0:T(1024)} %param.34) | copy-start | bytes 12292
  24.5 40.4 %copy-start.5 = (f32[16,2]{0,1:T(2,128)S(1)}, f32[16,2]{0,1:T(2,128)}, u32[]{:S(2)}) copy-start(f32[16,2]{0,1:T(2,128)} %param.36) | copy-start | bytes 388
  24.5 40.4 %copy-start.11 = (bf16[256]{0:T(256)(128)(2,1)S(1)}, bf16[256]{0:T(256)(128)(2,1)}, u32[]{:S(2)}) copy-start(bf16[256]{0:T(256)(128)(2,1)} %param.43) | copy-start | bytes 1540
  25.1 7.4 %all-to-all-start.1 = ((bf16[4,16,128]{2,1,0:T(8,128)(2,1)}), bf16[4,16,128]{2,1,0:T(8,128)(2,1)S(1)}, u32[]{:S(2)}, u32[]{:S(2)}) async-start(bf16[4,16,128]{2,1,0:T(8,128)(2,1)} %broadcast_in_dim.15), calls=%async_computation.1 | async-start | bytes 32768 | tf_op jit(solution)/shard_map/all_to_all | solution.py:14
  33.3 7.5 %all-to-all-start.2 = ((bf16[4,16,256]{2,1,0:T(8,128)(2,1)}), bf16[4,16,256]{2,1,0:T(8,128)(2,1)S(1)}, u32[]{:S(2)}, u32[]{:S(2)}) async-start(bf16[4,16,256]{2,1,0:T(8,128)(2,1)} %broadcast_in_dim.16), calls=%async_computation.2 | async-start | bytes 65536 | tf_op jit(solution)/shard_map/all_to_all | solution.py:14
  41.0 39.3 %copy-start.1 = (bf16[1,1024,352]{1,2,0:T(8,128)(2,1)S(1)}, bf16[1,1024,352]{1,2,0:T(8,128)(2,1)}, u32[]{:S(2)}) copy-start(bf16[1,1024,352]{1,2,0:T(8,128)(2,1)} %param.37) | copy-start | bytes 2162692
  42.6 38.1 %copy-start.6 = (bf16[1,352,1024]{2,1,0:T(8,128)(2,1)S(1)}, bf16[1,352,1024]{2,1,0:T(8,128)(2,1)}, u32[]{:S(2)}) copy-start(bf16[1,352,1024]{2,1,0:T(8,128)(2,1)} %param.39) | copy-start | bytes 2162692
  43.5 36.6 %all-to-all-start.3 = ((bf16[128,2,512]{2,1,0:T(2,128)(2,1)}), bf16[128,2,512]{2,1,0:T(2,128)(2,1)S(1)}, u32[]{:S(2)}, u32[]{:S(2)}) async-start(bf16[128,2,512]{2,1,0:T(2,128)(2,1)} %reshape.195), calls=%async_computation.3 | async-start | bytes 524288 | tf_op jit(solution)/shard_map/all_to_all | solution.py:133
  83.4 9.5 %all-to-all-start.4 = ((bf16[4,128,256]{2,1,0:T(8,128)(2,1)}), bf16[4,128,256]{2,1,0:T(8,128)(2,1)S(1)}, u32[]{:S(2)}, u32[]{:S(2)}) async-start(bf16[4,128,256]{2,1,0:T(8,128)(2,1)} %bitcast.113), calls=%async_computation.4 | async-start | bytes 524288 | tf_op jit(solution)/shard_map/all_to_all | solution.py:38
  93.5 7.3 %all-to-all-start.6 = ((bf16[4,1,16]{2,1,0:T(2,128)(2,1)}), bf16[4,1,16]{2,1,0:T(2,128)(2,1)S(1)}, u32[]{:S(2)}, u32[]{:S(2)}) async-start(bf16[4,1,16]{2,1,0:T(2,128)(2,1)} %broadcast_in_dim.18), calls=%async_computation.6 | async-start | bytes 4096 | tf_op jit(solution)/shard_map/all_to_all | solution.py:14
  100.7 19.3 %all-to-all-start.5 = ((bf16[128,2,128]{2,1,0:T(2,128)(2,1)}), bf16[128,2,128]{2,1,0:T(2,128)(2,1)S(1)}, u32[]{:S(2)}, u32[]{:S(2)}) async-start(bf16[128,2,128]{2,1,0:T(2,128)(2,1)} %reshape.197), calls=%async_computation.5 | async-start | bytes 131072 | tf_op jit(solution)/shard_map/all_to_all | solution.py:142
  120.8 11.0 %all-to-all-start.7 = ((bf16[4,16,3072]{2,1,0:T(8,128)(2,1)}), bf16[4,16,3072]{2,1,0:T(8,128)(2,1)S(1)}, u32[]{:S(2)}, u32[]{:S(2)}) async-start(bf16[4,16,3072]{2,1,0:T(8,128)(2,1)} %broadcast_in_dim.19), calls=%async_computation.7 | async-start | bytes 786432 | tf_op jit(solution)/shard_map/all_to_all | solution.py:14
  132.6 9.9 %all-to-all-start.8 = ((bf16[4,16,3072]{2,1,0:T(8,128)(2,1)}), bf16[4,16,3072]{2,1,0:T(8,128)(2,1)S(1)}, u32[]{:S(2)}, u32[]{:S(2)}) async-start(bf16[4,16,3072]{2,1,0:T(8,128)(2,1)} %broadcast_in_dim.20), calls=%async_computation.8 | async-start | bytes 786432 | tf_op jit(solution)/shard_map/all_to_all | solution.py:14
Sparse Core Ops, SparseCore 0:
  10.5 90.2 all-gather.2
  104.0 79.2 all-gather.4
where the time goes:
time: 193 us; the launch traced here: 192 us
  waiting for transfers between devices  96.8 us (50%)
  starting transfers between devices  54 us (28%)
  matrix products  14.1 us (7%)
  between operations  13.7 us (7%)
  local copies, waits for them, and re-layouts  9.37 us (5%)
  other arithmetic  4.49 us (2%)
    all_gather x1, waiting for transfers between devices, local(): lax.all_gather(dense_down, 'ep', axis=0, tiled=True)  40.6 us
    all_to_all x6, waiting for transfers between devices, sent_to_all(): lax.all_to_all(jnp.broadcast_to(shard[None], (size, *shard.shape)), axis,...  24.7 us
    all_to_all x6, starting transfers between devices, sent_to_all(): lax.all_to_all(jnp.broadcast_to(shard[None], (size, *shard.shape)), axis,...  21.5 us
    all_to_all x1, starting transfers between devices, local(): lax.all_to_all(outgoing, 'ep', split_axis=0, concat_axis=0, tiled=True)  21.3 us
    all_to_all x1, waiting for transfers between devices, local(): lax.all_to_all(outgoing, 'ep', split_axis=0, concat_axis=0, tiled=True)  15.1 us
    all_to_all x1, waiting for transfers between devices, local(): lax.all_to_all(summed.reshape(sources, item_count, -1), 'ep', split_axis=...  9.63 us
    all_to_all x1, starting transfers between devices, local(): lax.all_to_all(summed.reshape(sources, item_count, -1), 'ep', split_axis=...  7.71 us
    all_to_all x1, waiting for transfers between devices, sent_and_summed(): lax.all_to_all(blocks, axis, split_axis=0, concat_axis=0, tiled=True)  5.95 us
  transfers between devices with their start and end apart: 11, of which 10 were waited for; matrix products, arithmetic and copies ran while one was open for 13% of the time, Pallas kernels for 0%

commit v1 on v0

--- a/solution.py
+++ b/solution.py
@@ -162,7 +162,9 @@
     dense_hidden = (jax.nn.silu(gate_sum) * up_sum).astype(jnp.bfloat16)
     dense_out = jnp.dot(
         dense_hidden,
-        lax.all_gather(dense_down, "ep", axis=0, tiled=True),
+        jnp.concatenate(
+            lax.all_to_all(jnp.stack([dense_down] * lax.axis_size("ep")), "ep", 0, 0), axis=0
+        ),
         preferred_element_type=jnp.float32,
     )
     mix_gate = jax.nn.sigmoid(mix_logit)

time: 193 us -> 203 us (1.052)
  blocking collectives: 0 us -> 8.62 us
  waiting for transfers between devices: 96.8 us -> 89.5 us
  starting transfers between devices: 54 us -> 58.1 us
    all_gather x1 -> x0, waiting for transfers between devices: 40.6 us -> none  [local(): lax.all_gather(dense_down, 'ep', axis=0, tiled=True)]
    all_to_all x0 -> x1, waiting for transfers between devices: none -> 38.7 us  [local(): lax.all_to_all(jnp.stack([dense_down] * lax.axis_size('ep')), 'ep', 0, 0)]
    all_to_all x0 -> x1, blocking collectives: none -> 8.62 us  [sent_to_all(): lax.all_to_all(jnp.broadcast_to(shard[None], (size, *shard.shape)), axis,...]
    all_to_all x0 -> x1, starting transfers between devices: none -> 8.22 us  [local(): lax.all_to_all(jnp.stack([dense_down] * lax.axis_size('ep')), 'ep', 0, 0)]
    all_to_all x6 -> x5, waiting for transfers between devices: 24.7 us -> 18.8 us  [sent_to_all(): lax.all_to_all(jnp.broadcast_to(shard[None], (size, *shard.shape)), axis,...]
    all_to_all x6 -> x5, starting transfers between devices: 21.5 us -> 18 us  [sent_to_all(): lax.all_to_all(jnp.broadcast_to(shard[None], (size, *shard.shape)), axis,...]
  transfers between devices with their start and end apart: 11 -> 10, of which waited for: 10 -> 9; matrix products, arithmetic and copies ran while one was open for 13% -> 13% of each run, Pallas kernels for 0% -> 0%
where the time goes in v1:
time: 203 us; the launch traced here: 202 us
  waiting for transfers between devices  89.5 us (44%)
  starting transfers between devices  58.1 us (29%)
  matrix products  15.9 us (8%)
  between operations  13.7 us (7%)
  local copies, waits for them, and re-layouts  10.7 us (5%)
  blocking collectives  8.62 us (4%)
  other arithmetic  5.44 us (3%)
    all_to_all x1, waiting for transfers between devices, local(): lax.all_to_all(jnp.stack([dense_down] * lax.axis_size('ep')), 'ep', 0, 0)  38.7 us
    all_to_all x1, starting transfers between devices, local(): lax.all_to_all(outgoing, 'ep', split_axis=0, concat_axis=0, tiled=True)  21.3 us
    all_to_all x5, waiting for transfers between devices, sent_to_all(): lax.all_to_all(jnp.broadcast_to(shard[None], (size, *shard.shape)), axis,...  18.8 us
    all_to_all x5, starting transfers between devices, sent_to_all(): lax.all_to_all(jnp.broadcast_to(shard[None], (size, *shard.shape)), axis,...  18 us
    all_to_all x1, waiting for transfers between devices, local(): lax.all_to_all(outgoing, 'ep', split_axis=0, concat_axis=0, tiled=True)  15.9 us
    all_to_all x1, waiting for transfers between devices, local(): lax.all_to_all(summed.reshape(sources, item_count, -1), 'ep', split_axis=...  9.63 us
    all_to_all x1, blocking collectives, sent_to_all(): lax.all_to_all(jnp.broadcast_to(shard[None], (size, *shard.shape)), axis,...  8.62 us
    all_to_all x1, starting transfers between devices, local(): lax.all_to_all(jnp.stack([dense_down] * lax.axis_size('ep')), 'ep', 0, 0)  8.22 us
  transfers between devices with their start and end apart: 10, of which 9 were waited for; matrix products, arithmetic and copies ran while one was open for 13% of the time, Pallas kernels for 0%

profile of v1, /device:TPU:1, one launch (start us, length us, event | category | flops | bytes accessed | tf_op | source)
XLA Modules:
  0.0 201.9 jit_solution(18098796925456230521)
XLA Ops:
  6.5 1.4 pad_maximum_fusion
  8.0 1.3 broadcast_in_dim.14
  9.3 4.8 %all-to-all-start = ((bf16[4,16,256]{2,1,0:T(8,128)(2,1)}), bf16[4,16,256]{2,1,0:T(8,128)(2,1)S(1)}, u32[]{:S(2)}, u32[]{:S(2)}) async-start(bf16[4,16,256]{2,1,0:T(8,128)(2,1)} %broadcast_in_dim.14), calls=%async_computation | async-start | bytes 65536 | tf_op jit(solution)/shard_map/all_to_all | solution.py:14
  14.1 0.7 mul.148
  14.9 0.8 copy.72
  15.7 2.7 %all-to-all-done = bf16[4,16,256]{2,1,0:T(8,128)(2,1)S(1)} async-done(((bf16[4,16,256]{2,1,0:T(8,128)(2,1)}), bf16[4,16,256]{2,1,0:T(8,128)(2,1)S(1)}, u32[]{:S(2)}, u32[]{:S(2)}) %all-to-all-start) | async-done | bytes 32800 | tf_op jit(solution)/shard_map/all_to_all | solution.py:14
  18.7 0.8 multiply_convert_fusion.3
  19.5 1.2 fusion.51
  20.7 1.2 fusion.16
  21.9 0.8 bitcast_add_fusion
  22.7 0.8 maximum_bitcast_fusion
  23.6 1.1 fusion.14
  24.7 1.0 fusion.19
  25.8 0.6 broadcast_in_dim.15
  26.4 3.2 %all-to-all-start.1 = ((bf16[4,16,128]{2,1,0:T(8,128)(2,1)}), bf16[4,16,128]{2,1,0:T(8,128)(2,1)S(1)}, u32[]{:S(2)}, u32[]{:S(2)}) async-start(bf16[4,16,128]{2,1,0:T(8,128)(2,1)} %broadcast_in_dim.15), calls=%async_computation.1 | async-start | bytes 32768 | tf_op jit(solution)/shard_map/all_to_all | solution.py:14
  29.8 4.0 %all-to-all-done.1 = bf16[4,16,128]{2,1,0:T(8,128)(2,1)S(1)} async-done(((bf16[4,16,128]{2,1,0:T(8,128)(2,1)}), bf16[4,16,128]{2,1,0:T(8,128)(2,1)S(1)}, u32[]{:S(2)}, u32[]{:S(2)}) %all-to-all-start.1) | async-done | bytes 16416 | tf_op jit(solution)/shard_map/all_to_all | solution.py:14
  34.0 0.6 broadcast_in_dim.16
  34.6 3.3 %all-to-all-start.2 = ((bf16[4,16,256]{2,1,0:T(8,128)(2,1)}), bf16[4,16,256]{2,1,0:T(8,128)(2,1)S(1)}, u32[]{:S(2)}, u32[]{:S(2)}) async-start(bf16[4,16,256]{2,1,0:T(8,128)(2,1)} %broadcast_in_dim.16), calls=%async_computation.2 | async-start | bytes 65536 | tf_op jit(solution)/shard_map/all_to_all | solution.py:14
  38.1 4.1 %all-to-all-done.2 = bf16[4,16,256]{2,1,0:T(8,128)(2,1)S(1)} async-done(((bf16[4,16,256]{2,1,0:T(8,128)(2,1)}), bf16[4,16,256]{2,1,0:T(8,128)(2,1)S(1)}, u32[]{:S(2)}, u32[]{:S(2)}) %all-to-all-start.2) | async-done | bytes 32800 | tf_op jit(solution)/shard_map/all_to_all | solution.py:14
  42.7 0.6 broadcast.122
  43.3 0.8 reduce.9
  44.1 0.9 reshape.201
  45.0 21.3 %all-to-all-start.3 = ((bf16[128,2,512]{2,1,0:T(2,128)(2,1)}), bf16[128,2,512]{2,1,0:T(2,128)(2,1)S(1)}, u32[]{:S(2)}, u32[]{:S(2)}) async-start(bf16[128,2,512]{2,1,0:T(2,128)(2,1)} %reshape.201), calls=%async_computation.3 | async-start | bytes 524288 | tf_op jit(solution)/shard_map/all_to_all | solution.py:133
  66.4 15.9 %all-to-all-done.3 = bf16[128,2,512]{2,1,0:T(2,128)(2,1)S(1)} async-done(((bf16[128,2,512]{2,1,0:T(2,128)(2,1)}), bf16[128,2,512]{2,1,0:T(2,128)(2,1)S(1)}, u32[]{:S(2)}, u32[]{:S(2)}) %all-to-all-start.3) | async-done | bytes 262176 | tf_op jit(solution)/shard_map/all_to_all | solution.py:133
  82.9 2.0 convolution_convert_fusion.3
  84.9 0.7 copy.109
  85.7 3.4 %all-to-all-start.4 = ((bf16[4,128,256]{2,1,0:T(8,128)(2,1)}), bf16[4,128,256]{2,1,0:T(8,128)(2,1)S(1)}, u32[]{:S(2)}, u32[]{:S(2)}) async-start(bf16[4,128,256]{2,1,0:T(8,128)(2,1)} %bitcast.114), calls=%async_computation.4 | async-start | bytes 524288 | tf_op jit(solution)/shard_map/all_to_all | solution.py:38
  89.2 6.5 %all-to-all-done.4 = bf16[4,128,256]{2,1,0:T(8,128)(2,1)S(1)} async-done(((bf16[4,128,256]{2,1,0:T(8,128)(2,1)}), bf16[4,128,256]{2,1,0:T(8,128)(2,1)S(1)}, u32[]{:S(2)}, u32[]{:S(2)}) %all-to-all-start.4) | async-done | bytes 262176 | tf_op jit(solution)/shard_map/all_to_all | solution.py:38
  95.7 0.6 broadcast_in_dim.18
  96.3 3.2 %all-to-all-start.6 = ((bf16[4,1,16]{2,1,0:T(2,128)(2,1)}), bf16[4,1,16]{2,1,0:T(2,128)(2,1)S(1)}, u32[]{:S(2)}, u32[]{:S(2)}) async-start(bf16[4,1,16]{2,1,0:T(2,128)(2,1)} %broadcast_in_dim.18), calls=%async_computation.6 | async-start | bytes 4096 | tf_op jit(solution)/shard_map/all_to_all | solution.py:14
  99.5 0.7 reduce.10
  100.3 0.6 reshape.203
  100.9 2.6 %all-to-all-done.6 = bf16[4,1,16]{2,1,0:T(2,128)(2,1)S(1)} async-done(((bf16[4,1,16]{2,1,0:T(2,128)(2,1)}), bf16[4,1,16]{2,1,0:T(2,128)(2,1)S(1)}, u32[]{:S(2)}, u32[]{:S(2)}) %all-to-all-start.6) | async-done | bytes 160 | tf_op jit(solution)/shard_map/all_to_all | solution.py:14
  103.5 7.2 %all-to-all-start.5 = ((bf16[128,2,128]{2,1,0:T(2,128)(2,1)}), bf16[128,2,128]{2,1,0:T(2,128)(2,1)S(1)}, u32[]{:S(2)}, u32[]{:S(2)}) async-start(bf16[128,2,128]{2,1,0:T(2,128)(2,1)} %reshape.203), calls=%async_computation.5 | async-start | bytes 131072 | tf_op jit(solution)/shard_map/all_to_all | solution.py:142
  110.7 1.9 convolution_convert_fusion
  112.7 9.6 %all-to-all-done.5 = bf16[128,2,128]{2,1,0:T(2,128)(2,1)S(1)} async-done(((bf16[128,2,128]{2,1,0:T(2,128)(2,1)}), bf16[128,2,128]{2,1,0:T(2,128)(2,1)S(1)}, u32[]{:S(2)}, u32[]{:S(2)}) %all-to-all-start.5) | async-done | bytes 65568 | tf_op jit(solution)/shard_map/all_to_all | solution.py:142
  122.3 0.8 broadcast_in_dim.20
  123.1 3.5 %all-to-all-start.8 = ((bf16[4,16,3072]{2,1,0:T(8,128)(2,1)}), bf16[4,16,3072]{2,1,0:T(8,128)(2,1)S(1)}, u32[]{:S(2)}, u32[]{:S(2)}) async-start(bf16[4,16,3072]{2,1,0:T(8,128)(2,1)} %broadcast_in_dim.20), calls=%async_computation.8 | async-start | bytes 786432 | tf_op jit(solution)/shard_map/all_to_all | solution.py:14
  126.5 1.9 convolution_convert_fusion.1
  128.5 5.3 %all-to-all-done.8 = bf16[4,16,3072]{2,1,0:T(8,128)(2,1)S(1)} async-done(((bf16[4,16,3072]{2,1,0:T(8,128)(2,1)}), bf16[4,16,3072]{2,1,0:T(8,128)(2,1)S(1)}, u32[]{:S(2)}, u32[]{:S(2)}) %all-to-all-start.8) | async-done | bytes 393248 | tf_op jit(solution)/shard_map/all_to_all | solution.py:14
  133.8 8.6 %all_to_all.51 = bf16[4,16,3072]{2,1,0:T(8,128)(2,1)S(1)} all-to-all(bf16[4,16,3072]{2,1,0:T(8,128)(2,1)S(1)} %broadcast_in_dim.19), channel_id=1, replica_groups=mesh['ep'=128,'tp'=4] {'tp'}, dimensions={0} | all-to-all | bytes 786432 | tf_op jit(solution)/shard_map/all_to_all | solution.py:14
  142.4 1.3 stack.2
  143.7 8.2 %all-to-all-start.9 = ((bf16[128,24,256]{2,1,0:T(8,128)(2,1)}), bf16[128,24,256]{2,1,0:T(8,128)(2,1)S(1)}, u32[]{:S(2)}, u32[]{:S(2)}) async-start(bf16[128,24,256]{2,1,0:T(8,128)(2,1)} %stack.2), calls=%async_computation.9 | async-start | bytes 3145728 | tf_op jit(solution)/shard_map/all_to_all | solution.py:166
  152.1 0.7 reshape.204
  152.8 1.0 fusion.4
  153.8 0.8 convert_reduce_fusion
  154.6 38.7 %all-to-all-done.9 = bf16[128,24,256]{2,1,0:T(8,128)(2,1)S(1)} async-done(((bf16[128,24,256]{2,1,0:T(8,128)(2,1)}), bf16[128,24,256]{2,1,0:T(8,128)(2,1)S(1)}, u32[]{:S(2)}, u32[]{:S(2)}) %all-to-all-start.9) | async-done | bytes 1572896 | tf_op jit(solution)/shard_map/all_to_all | solution.py:166
  193.2 1.8 fusion.7
  (57 shorter events, 2.5 us)
Async XLA Ops:
  6.5 18.1 %copy-start = (f32[16,1,128,128]{3,2,1,0:T(8,128)S(1)}, f32[16,1,128,128]{3,2,1,0:T(8,128)}, u32[]{:S(2)}) copy-start(f32[16,1,128,128]{3,2,1,0:T(8,128)} %param.31) | copy-start | bytes 3145732
  6.5 19.1 %copy-start.8 = (bf16[1024,128]{1,0:T(8,128)(2,1)S(1)}, bf16[1024,128]{1,0:T(8,128)(2,1)}, u32[]{:S(2)}) copy-start(bf16[1024,128]{1,0:T(8,128)(2,1)} %param.26) | copy-start | bytes 786436
  6.5 104.2 %all-gather.2.cloned.1.call-start = ((), (), s32[]{:S(2)}) async-start(), calls=%async_computation.10 | async-start | bytes 3170304 | tf_op jit(solution)/shard_map/all_gather | solution.py:46
  9.3 9.1 %all-to-all-start = ((bf16[4,16,256]{2,1,0:T(8,128)(2,1)}), bf16[4,16,256]{2,1,0:T(8,128)(2,1)S(1)}, u32[]{:S(2)}, u32[]{:S(2)}) async-start(bf16[4,16,256]{2,1,0:T(8,128)(2,1)} %broadcast_in_dim.14), calls=%async_computation | async-start | bytes 65536 | tf_op jit(solution)/shard_map/all_to_all | solution.py:14
  14.1 19.7 %copy-start.2 = (bf16[512,256]{1,0:T(8,128)(2,1)S(1)}, bf16[512,256]{1,0:T(8,128)(2,1)}, u32[]{:S(2)}) copy-start(bf16[512,256]{1,0:T(8,128)(2,1)} %param.30) | copy-start | bytes 786436
  14.1 19.7 %copy-start.3 = (bf16[16,256]{1,0:T(8,128)(2,1)S(1)}, bf16[16,256]{1,0:T(8,128)(2,1)}, u32[]{:S(2)}) copy-start(bf16[16,256]{1,0:T(8,128)(2,1)} %param.22) | copy-start | bytes 24580
  19.4 22.9 %copy-start.5 = (f32[1024]{0:T(1024)S(1)}, f32[1024]{0:T(1024)}, u32[]{:S(2)}) copy-start(f32[1024]{0:T(1024)} %param.34) | copy-start | bytes 12292
  25.8 40.6 %copy-start.9 = (bf16[256]{0:T(256)(128)(2,1)S(1)}, bf16[256]{0:T(256)(128)(2,1)}, u32[]{:S(2)}) copy-start(bf16[256]{0:T(256)(128)(2,1)} %param.43) | copy-start | bytes 1540
  26.4 7.4 %all-to-all-start.1 = ((bf16[4,16,128]{2,1,0:T(8,128)(2,1)}), bf16[4,16,128]{2,1,0:T(8,128)(2,1)S(1)}, u32[]{:S(2)}, u32[]{:S(2)}) async-start(bf16[4,16,128]{2,1,0:T(8,128)(2,1)} %broadcast_in_dim.15), calls=%async_computation.1 | async-start | bytes 32768 | tf_op jit(solution)/shard_map/all_to_all | solution.py:14
  34.6 7.5 %all-to-all-start.2 = ((bf16[4,16,256]{2,1,0:T(8,128)(2,1)}), bf16[4,16,256]{2,1,0:T(8,128)(2,1)S(1)}, u32[]{:S(2)}, u32[]{:S(2)}) async-start(bf16[4,16,256]{2,1,0:T(8,128)(2,1)} %broadcast_in_dim.16), calls=%async_computation.2 | async-start | bytes 65536 | tf_op jit(solution)/shard_map/all_to_all | solution.py:14
  42.2 40.3 %copy-start.1 = (bf16[1,1024,352]{1,2,0:T(8,128)(2,1)S(1)}, bf16[1,1024,352]{1,2,0:T(8,128)(2,1)}, u32[]{:S(2)}) copy-start(bf16[1,1024,352]{1,2,0:T(8,128)(2,1)} %param.37) | copy-start | bytes 2162692
  44.1 38.8 %copy-start.7 = (bf16[1,352,1024]{2,1,0:T(8,128)(2,1)S(1)}, bf16[1,352,1024]{2,1,0:T(8,128)(2,1)}, u32[]{:S(2)}) copy-start(bf16[1,352,1024]{2,1,0:T(8,128)(2,1)} %param.39) | copy-start | bytes 2162692
  45.0 37.2 %all-to-all-start.3 = ((bf16[128,2,512]{2,1,0:T(2,128)(2,1)}), bf16[128,2,512]{2,1,0:T(2,128)(2,1)S(1)}, u32[]{:S(2)}, u32[]{:S(2)}) async-start(bf16[128,2,512]{2,1,0:T(2,128)(2,1)} %reshape.201), calls=%async_computation.3 | async-start | bytes 524288 | tf_op jit(solution)/shard_map/all_to_all | solution.py:133
  85.7 10.0 %all-to-all-start.4 = ((bf16[4,128,256]{2,1,0:T(8,128)(2,1)}), bf16[4,128,256]{2,1,0:T(8,128)(2,1)S(1)}, u32[]{:S(2)}, u32[]{:S(2)}) async-start(bf16[4,128,256]{2,1,0:T(8,128)(2,1)} %bitcast.114), calls=%async_computation.4 | async-start | bytes 524288 | tf_op jit(solution)/shard_map/all_to_all | solution.py:38
  96.3 7.3 %all-to-all-start.6 = ((bf16[4,1,16]{2,1,0:T(2,128)(2,1)}), bf16[4,1,16]{2,1,0:T(2,128)(2,1)S(1)}, u32[]{:S(2)}, u32[]{:S(2)}) async-start(bf16[4,1,16]{2,1,0:T(2,128)(2,1)} %broadcast_in_dim.18), calls=%async_computation.6 | async-start | bytes 4096 | tf_op jit(solution)/shard_map/all_to_all | solution.py:14
  103.5 18.8 %all-to-all-start.5 = ((bf16[128,2,128]{2,1,0:T(2,128)(2,1)}), bf16[128,2,128]{2,1,0:T(2,128)(2,1)S(1)}, u32[]{:S(2)}, u32[]{:S(2)}) async-start(bf16[128,2,128]{2,1,0:T(2,128)(2,1)} %reshape.203), calls=%async_computation.5 | async-start | bytes 131072 | tf_op jit(solution)/shard_map/all_to_all | solution.py:142
  123.1 10.7 %all-to-all-start.8 = ((bf16[4,16,3072]{2,1,0:T(8,128)(2,1)}), bf16[4,16,3072]{2,1,0:T(8,128)(2,1)S(1)}, u32[]{:S(2)}, u32[]{:S(2)}) async-start(bf16[4,16,3072]{2,1,0:T(8,128)(2,1)} %broadcast_in_dim.20), calls=%async_computation.8 | async-start | bytes 786432 | tf_op jit(solution)/shard_map/all_to_all | solution.py:14
  126.5 15.9 %copy-start.4 = (bf16[24,256]{1,0:T(8,128)(2,1)S(1)}, bf16[24,256]{1,0:T(8,128)(2,1)}, u32[]{:S(2)}) copy-start(bf16[24,256]{1,0:T(8,128)(2,1)} %param.42) | copy-start | bytes 36868
  143.7 8.2 %copy-start.6 = (f32[16,2]{0,1:T(2,128)S(1)}, f32[16,2]{0,1:T(2,128)}, u32[]{:S(2)}) copy-start(f32[16,2]{0,1:T(2,128)} %param.36) | copy-start | bytes 388
  143.7 49.5 %all-to-all-start.9 = ((bf16[128,24,256]{2,1,0:T(8,128)(2,1)}), bf16[128,24,256]{2,1,0:T(8,128)(2,1)S(1)}, u32[]{:S(2)}, u32[]{:S(2)}) async-start(bf16[128,24,256]{2,1,0:T(8,128)(2,1)} %stack.2), calls=%async_computation.9 | async-start | bytes 3145728 | tf_op jit(solution)/shard_map/all_to_all | solution.py:166
Sparse Core Ops, SparseCore 0:
  10.5 91.1 all-gather.1
